TPU v7x, 256 devices: a whole 4x4x8 slice. The times are simulated.
256 devices in a mesh: sp: 16 (over y, x), tp: 16 (over z, core).
Axes of the slice: x: 4, y: 4, z: 8, core: 2. Of those that a mesh axis runs over, the one named last changes fastest.
Arguments:
- query_rows: bfloat16 [65536, 1024], P('sp', 'tp'), may hold values from -6 to 6
- key_rows: bfloat16 [65536, 1024], P('sp', 'tp'), may hold values from -6 to 6
- value_rows: bfloat16 [65536, 1024], P('sp', 'tp'), may hold values from -6 to 6
- gate_rows: bfloat16 [65536, 1024], P('sp', 'tp'), may hold values from -6 to 6
- log_decay: float32 [16, 65536], P('tp', 'sp'), may hold values from -1 to 0
- residual: bfloat16 [65536, 2048], P(('sp', 'tp')), may hold values from -6 to 6
- head_gain: float32 [1024], P('tp'), may hold values from 0.1 to 1.9
- out_weight: bfloat16 [1024, 2048], P(None, 'tp'), may hold values from -0.1875 to 0.1875
- norm_gain: float32 [2048], replicated, may hold values from 0.1 to 1.9
- expert_ids: int32 [65536, 2], P(('sp', 'tp')), may hold values from 0 to 15, all different within a row; in each aligned block of 256 rows (0 to 255, 256 to 511, ...) at most 48 rows name the same one
- route_weights: float32 [65536, 2], P(('sp', 'tp')), may hold values from 0.2 to 1
- expert_gate: bfloat16 [2048, 16384], P(None, ('sp', 'tp')), may hold values from -0.125 to 0.125
- expert_up: bfloat16 [2048, 16384], P(None, ('sp', 'tp')), may hold values from -0.125 to 0.125
- expert_down: bfloat16 [2048, 16384], P(None, ('sp', 'tp')), may hold values from -0.1875 to 0.1875
- shared_gate: bfloat16 [2048, 512], replicated, may hold values from -0.125 to 0.125
- shared_up: bfloat16 [2048, 512], replicated, may hold values from -0.125 to 0.125
- shared_down: bfloat16 [2048, 512], replicated, may hold values from -0.25 to 0.25
Outputs:
- result: bfloat16 [65536, 2048], P(('sp', 'tp'))
Inputs may be any that keep to these rules, and one draw needn't show every extreme that they name: `expert_ids`: each row names 2 different experts. Within the rows of one device (aligned blocks of 256 rows) no expert is named by more than 48 rows, and in some block an expert is named by exactly 48 rows.
All inputs are finite; a program needn't handle non-finite values.
Results may differ from a plain program's by a relative error of at most 0.0075.
Values may be sent and summed in bfloat16 or wider, within the bound.
No kernel may reach another device: no remote copies, remote signals or barrier semaphores. Data moves between devices by JAX's collectives and lax.ppermute only.
A program may use at most 128 MiB of HBM per device.

v0:
```python
import jax
import jax.numpy as jnp
from jax import lax
from jax.sharding import PartitionSpec as P

HEAD = 64
SPAN = 512


eps = 1e-05


def sent_to_all(value, axis):
    length = lax.axis_size(axis)
    return lax.all_to_all(
        jnp.broadcast_to(value[None], (length, *value.shape)), axis, 0, 0, tiled=True
    )


def all_in_one(value, axis):
    leaves = jax.tree.leaves(value)
    order = sorted(range(len(leaves)), key=lambda k: -leaves[k].size)
    width = (1, *leaves[order[0]].shape)[-1]
    lines = [
        jnp.pad(leaves[k].reshape(-1), (0, -leaves[k].size % width)).reshape(-1, width)
        for k in order
    ]
    both, at, found = (sent_to_all(jnp.concatenate(lines), axis), 0, {})
    for k, line in zip(order, lines):
        share = both[:, at : at + len(line)].reshape(len(both), -1)
        found[k] = share[:, : leaves[k].size].reshape(-1, *leaves[k].shape)
        at += len(line)
    numbers = iter(range(len(leaves)))
    return jax.tree.map(lambda _: found[next(numbers)], value)


def joined_by_halves(pieces, combine):
    while len(jax.tree.leaves(pieces)[0]) > 1:
        pieces = jax.vmap(combine)(
            *(jax.tree.map(lambda part: part[side::2], pieces) for side in (0, 1))
        )
    return jax.tree.map(lambda part: part[0], pieces)


def carried_in(value, axis, combine, identity):
    length, place = (lax.axis_size(axis), lax.axis_index(axis))
    passed = jnp.arange(length) < place

    def kept(part, zero, own):
        part = jnp.where(
            passed.reshape(-1, *(1 for _ in own.shape)), part, jnp.asarray(zero, own.dtype)
        )
        return part

    pieces = all_in_one(value, axis)
    return joined_by_halves(jax.tree.map(kept, pieces, identity, value), combine)


def side_by_side(arrays, axis, dim, along):
    both = jnp.concatenate(arrays, axis=along)
    filled, at, done = (lax.all_gather(both, axis, axis=dim, tiled=True), 0, [])
    for a in arrays:
        done.append(lax.slice_in_dim(filled, at, at + a.shape[along], axis=along))
        at += a.shape[along]
    return tuple(done)


def block_pass(queries, key_heads, values, log_decay, state):
    rows, heads, width = queries.shape
    count = rows // SPAN
    scale = width ** (-0.5)
    query_blocks = queries.reshape(count, SPAN, heads, width)
    key_blocks = key_heads.reshape(count, SPAN, heads, width)
    value_blocks = values.reshape(count, SPAN, heads, width)
    decay_blocks = log_decay.reshape(heads, count, SPAN).transpose(1, 0, 2)
    offsets = jnp.arange(SPAN, dtype=jnp.int32)
    causal = offsets[:, None] >= offsets[None, :]

    def advance(carry, inputs):
        block_queries, block_keys, block_values, decay_block = inputs
        running = jnp.cumsum(decay_block, axis=1)
        spread = running[:, :, None] - running[:, None, :]
        damping = jnp.exp(jnp.where(causal[None], spread, -jnp.inf))
        attention_scores = jnp.einsum(
            "xru,jru->rxj", block_queries, block_keys, preferred_element_type=jnp.float32
        )
        decay_weighted = (attention_scores * scale * damping).astype(jnp.bfloat16)
        inner_block_term = jnp.einsum(
            "svc,csj->vsj", decay_weighted, block_values, preferred_element_type=jnp.float32
        )
        carried = jnp.einsum(
            "nhd,hde->nhe",
            block_queries.astype(jnp.float32),
            carry,
            precision=lax.Precision.HIGHEST,
        )
        carried = carried * jnp.exp(running).T[:, :, None]
        decay_to_block_end = jnp.exp(running[:, -1:] - running).T[:, :, None] * scale
        state_update = jnp.einsum(
            "jok,jow->okw",
            block_keys.astype(jnp.float32) * decay_to_block_end,
            block_values.astype(jnp.float32),
            precision=lax.Precision.HIGHEST,
        )
        carry = carry * jnp.exp(running[:, -1])[:, None, None] + state_update
        return (carry, inner_block_term + carried)

    final, outputs = lax.scan(
        advance, state, (query_blocks, key_blocks, value_blocks, decay_blocks)
    )
    return (final, outputs.reshape(rows, heads, width))


def combine_states(earlier, later):
    return (earlier[0] * later[0], earlier[1] * later[0][:, None, None] + later[1])


def entering_state(totals, own_state):
    identity = (jnp.ones_like(totals), jnp.zeros_like(own_state))
    return carried_in((totals, own_state), "sp", combine_states, identity)[1]


def on_device(
    query_rows,
    key_rows,
    value_rows,
    gate_rows,
    log_decay,
    residual,
    head_gain,
    out_weight,
    norm_gain,
    expert_ids,
    route_weights,
    expert_gate,
    expert_up,
    expert_down,
    shared_gate,
    shared_up,
    shared_down,
):
    seq_rows, local_width = query_rows.shape
    heads = local_width // HEAD
    out_full, gate_full, up_full, down_full = (
        lax.all_gather(out_weight, "tp", axis=1, tiled=True),
        *side_by_side((expert_gate, expert_up, expert_down), "tp", 1, 0),
    )
    queries = query_rows.reshape(seq_rows, heads, HEAD)
    key_heads = key_rows.reshape(seq_rows, heads, HEAD)
    values = value_rows.reshape(seq_rows, heads, HEAD)
    running = jnp.cumsum(log_decay, axis=1)
    totals = jnp.exp(running[:, -1])
    decay_to_block_end = (jnp.exp(running[:, -1:] - running).T * HEAD ** (-0.5))[:, :, None]
    own_state = jnp.einsum(
        "jok,jow->okw",
        key_heads.astype(jnp.float32) * decay_to_block_end,
        values.astype(jnp.float32),
        precision=lax.Precision.HIGHEST,
    )
    incoming = entering_state(totals, own_state)
    _, retained = block_pass(queries, key_heads, values, log_decay, incoming)
    centered = retained - jnp.mean(retained, axis=2, keepdims=True)
    normed = centered * lax.rsqrt(jnp.mean(centered * centered, axis=2, keepdims=True) + eps)
    ret_rows = (
        normed.reshape(seq_rows, local_width)
        * head_gain
        * jax.nn.silu(gate_rows.astype(jnp.float32))
    ).astype(jnp.bfloat16)
    token_rows = lax.all_to_all(ret_rows, "tp", split_axis=0, concat_axis=1, tiled=True)
    mixer = jnp.dot(token_rows, out_full, preferred_element_type=jnp.float32)
    hidden = (residual.astype(jnp.float32) + mixer).astype(jnp.bfloat16)
    hidden_wide = hidden.astype(jnp.float32)
    normed_rows = (
        hidden_wide
        * lax.rsqrt(jnp.mean(hidden_wide * hidden_wide, axis=1, keepdims=True) + eps)
        * norm_gain
    ).astype(jnp.bfloat16)
    shared_mid = (
        jax.nn.silu(jnp.dot(normed_rows, shared_gate, preferred_element_type=jnp.float32))
        * jnp.dot(normed_rows, shared_up, preferred_element_type=jnp.float32)
    ).astype(jnp.bfloat16)
    shared_out = lax.dot_general(
        shared_mid, shared_down, (((1,), (1,)), ((), ())), preferred_element_type=jnp.float32
    )
    specialist_networks = lax.axis_size("sp")
    token_count, chosen_count = expert_ids.shape
    model_width = normed_rows.shape[1]
    capacity = 3 * token_count * chosen_count // (2 * specialist_networks)
    flat_ids = expert_ids.reshape(-1)
    matches = (
        flat_ids[:, None] == jnp.arange(specialist_networks, dtype=jnp.int32)[None, :]
    ).astype(jnp.int32)
    position = jnp.sum((jnp.cumsum(matches, axis=0) - 1) * matches, axis=1)
    slot = flat_ids * capacity + position
    owner = jnp.arange(token_count * chosen_count, dtype=jnp.int32) // chosen_count
    slot_token = jnp.zeros((specialist_networks * capacity,), jnp.int32).at[slot].set(owner)
    slot_live = jnp.zeros((specialist_networks * capacity,), jnp.bfloat16).at[slot].set(1.0)
    outgoing = (normed_rows[slot_token] * slot_live[:, None]).reshape(
        specialist_networks, capacity, model_width
    )
    arrived = lax.all_to_all(outgoing, "sp", split_axis=0, concat_axis=0, tiled=True)
    flat_rows = arrived.reshape(-1, model_width)
    middle = (
        jax.nn.silu(jnp.dot(flat_rows, gate_full, preferred_element_type=jnp.float32))
        * jnp.dot(flat_rows, up_full, preferred_element_type=jnp.float32)
    ).astype(jnp.bfloat16)
    outcome = lax.dot_general(
        middle, down_full, (((1,), (1,)), ((), ())), preferred_element_type=jnp.float32
    ).astype(jnp.bfloat16)
    processed = outcome.reshape(arrived.shape)
    returned = lax.all_to_all(processed, "sp", split_axis=0, concat_axis=0, tiled=True)
    picked = returned.reshape(specialist_networks * capacity, model_width)[slot].astype(jnp.float32)
    decay_weighted = picked * route_weights.reshape(-1)[:, None]
    routed = jnp.sum(decay_weighted.reshape(token_count, chosen_count, model_width), axis=1)
    return (hidden_wide + routed + shared_out).astype(jnp.bfloat16)


def solution(mesh):
    placed = (
        P("sp", "tp"),
        P("sp", "tp"),
        P("sp", "tp"),
        P("sp", "tp"),
        P("tp", "sp"),
        P(("sp", "tp"), None),
        P("tp"),
        P(None, "tp"),
        P(),
        P(("sp", "tp"), None),
        P(("sp", "tp"), None),
        P(None, ("sp", "tp")),
        P(None, ("sp", "tp")),
        P(None, ("sp", "tp")),
        P(),
        P(),
        P(),
    )
    return jax.shard_map(
        on_device, mesh=mesh, in_specs=placed, out_specs=P(("sp", "tp"), None), check_vma=False
    )
```

profile of v0, /device:TPU:1, one launch (start us, length us, event | category | flops | bytes accessed | tf_op | source)
XLA Modules:
  0.0 287.4 jit_solution(11375161928984603023)
XLA Ops:
  7.3 2.0 pad_maximum_fusion
  14.4 7.6 %all-to-all-start = ((f32[16,65,64]{1,2,0:T(8,128)}), f32[16,65,64]{1,2,0:T(8,128)}, u32[]{:S(2)}, u32[]{:S(2)}) async-start(f32[16,65,64]{1,2,0:T(8,128)} %broadcast_in_dim.39), calls=%async_computation | async-start | bytes 1048576 | tf_op jit(solution)/shard_map/all_to_all | solution.py:15
  22.5 1.3 copy.64
  27.1 1.1 reduce-window.26
  28.5 4.0 %all-to-all-done = f32[16,65,64]{1,2,0:T(8,128)} async-done(((f32[16,65,64]{1,2,0:T(8,128)}), f32[16,65,64]{1,2,0:T(8,128)}, u32[]{:S(2)}, u32[]{:S(2)}) %all-to-all-start) | async-done | bytes 266272 | tf_op jit(solution)/shard_map/all_to_all | solution.py:15
  32.5 2.0 slice.131
  34.6 1.2 copy.61
  36.8 1.1 fusion.69
  39.0 56.5 %while.13 = (s32[]{:T(128)}, f32[1,64,64]{2,1,0:T(8,128)S(1)}, f32[8,512,1,64]{1,3,2,0:T(8,128)S(1)}, f32[8,1,512]{2,1,0:T(1,128)S(1)}, bf16[8,512,1,64]{1,3,2,0...) while((s32[]{:T(128)}, f32[1,64,64]{2,1,0:T(8,128)S(1)}, ...), condition=%wide.region_5.6_spmd.clone, body=%wide.region_2.5_spmd.clone.sunk | while | flops 119219216 | bytes 885013 | solution.py:108
  39.7 1.5 fusion.130
  41.2 1.1 fusion.131
  46.8 1.5 fusion.130
  48.3 1.1 fusion.131
  52.0 1.1 fusion.129
  53.9 1.5 fusion.130
  55.3 1.1 fusion.131
  60.9 1.5 fusion.130
  62.4 1.1 fusion.131
  67.9 1.4 fusion.130
  69.4 1.1 fusion.131
  73.1 1.1 fusion.129
  75.0 1.5 fusion.130
  76.5 1.1 fusion.131
  80.2 1.1 fusion.129
  82.1 1.5 fusion.130
  83.5 1.1 fusion.131
  89.1 1.5 fusion.130
  90.6 1.1 fusion.131
  94.3 1.1 fusion.129
  97.9 10.5 %all-to-all-start.1 = ((bf16[16,256,64]{1,2,0:T(8,128)(2,1)}), bf16[16,256,64]{1,2,0:T(8,128)(2,1)S(1)}, u32[]{:S(2)}, u32[]{:S(2)}) async-start(bf16[16,256,64]{1,2,0:T(8,128)(2,1)} %bitcast.155), calls=%async_computation.1 | async-start | bytes 1048576 | tf_op jit(solution)/shard_map/all_to_all | solution.py:169
  108.8 2.4 scatter_custom_fusion
  111.3 3.9 %scatter_custom_fusion.1 = bf16[768]{0:T(1024)(128)(2,1)S(1)} fusion(s32[512]{0:T(512)S(1)} %bitcast.220, bf16[512]{0:T(512)(128)(2,1)S(1)} %broadcast.246, bf16[]{:T(256)} %constant.89.clone.1), kind=kCustom, calls=%fused_computation.132 | custom fusion | bytes 1538 | tf_op jit(solution)/shard_map/scatter | solution.py:197
  115.3 15.4 %all-to-all-done.1 = bf16[16,256,64]{1,2,0:T(8,128)(2,1)S(1)} async-done(((bf16[16,256,64]{1,2,0:T(8,128)(2,1)}), bf16[16,256,64]{1,2,0:T(8,128)(2,1)S(1)}, u32[]{:S(2)}, u32[]{:S(2)}) %all-to-all-start.1) | async-done | bytes 524320 | tf_op jit(solution)/shard_map/all_to_all | solution.py:169
  130.7 4.0 %fusion.55 = (f32[256]{0:T(256)S(1)}, bf16[256,2048]{1,0:T(8,128)(2,1)S(1)}) fusion(bf16[256,1024]{0,1:T(8,128)(2,1)S(1)} %bitcast.207, bf16[1024,2048]{1,0:T(8,128)(2,1)} %all-gather.3.cloned.1.call-done, bf16[256,2048]{1,0:T(8,128)(2,1)} %param.24), kind=kOutput, calls=%fused_computation.67 | convolution fusion | flops 1076887296 | bytes 6816768 | tf_op jit(solution)/shard_map/dot_general | solution.py:170
  136.0 4.3 %gather_fusion = bf16[768,2048]{1,0:T(8,128)(2,1)} fusion(bf16[256,2048]{1,0:T(8,128)(2,1)S(1)} %fusion.57, s32[1024]{0:T(1024)S(1)} %pad_clamp_fusion.1), kind=kCustom, calls=%fused_computation | custom fusion | bytes 6294528 | tf_op jit(solution)/shard_map/gather | solution.py:198
  140.4 2.2 broadcast_multiply_fusion
  142.5 42.9 %all_to_all.34 = bf16[16,48,2048]{2,1,0:T(8,128)(2,1)} all-to-all(bf16[16,48,2048]{2,1,0:T(8,128)(2,1)S(1)} %broadcast_multiply_fusion), channel_id=1, replica_groups=mesh['sp'=16,'tp'=16] {'sp'}, dimensions={0} | all-to-all | bytes 6291456 | tf_op jit(solution)/shard_map/all_to_all | solution.py:201
  185.5 6.4 %fusion.46 = f32[768,1024]{1,0:T(8,128)S(1)} fusion(bf16[768,2048]{1,0:T(8,128)(2,1)} %bitcast.198, bf16[6144,1024]{0,1:T(8,128)(2,1)} %all-gather.5.cloned.1.call-done), kind=kOutput, calls=%fused_computation.53 | convolution fusion | flops 3221225472 | bytes 10485760 | tf_op jit(solution)/shard_map/dot_general | solution.py:205
  191.8 1.3 copy-done.15
  193.2 3.9 %multiply_convert_fusion = bf16[768,1024]{1,0:T(8,128)(2,1)S(1)} fusion(f32[768,1024]{1,0:T(8,128)S(1)} %fusion.46, bf16[768,2048]{1,0:T(8,128)(2,1)S(1)} %bitcast.199, bf16[6144,1024]{0,1:T(8,128)(2,1)S(1)} %copy-done.15), kind=kOutput, calls=%fused_computation.59 | convolution fusion | flops 3225944064 | bytes 12058624 | tf_op jit(solution)/shard_map/dot_general | solution.py:204
  197.0 4.9 %fusion.50 = bf16[768,2048]{1,0:T(8,128)(2,1)} fusion(bf16[768,1024]{1,0:T(8,128)(2,1)S(1)} %multiply_convert_fusion, bf16[6144,1024]{0,1:T(8,128)(2,1)S(1)} %copy-done.15), kind=kOutput, calls=%fused_computation.58 | convolution fusion | flops 3222798336 | bytes 8912896 | tf_op jit(solution)/shard_map/dot_general | solution.py:207
  201.9 4.8 %all-to-all-start.3 = ((bf16[16,48,2048]{2,1,0:T(8,128)(2,1)}), bf16[16,48,2048]{2,1,0:T(8,128)(2,1)}, u32[]{:S(2)}, u32[]{:S(2)}) async-start(bf16[16,48,2048]{2,1,0:T(8,128)(2,1)} %bitcast.197), calls=%async_computation.3 | async-start | bytes 6291456 | tf_op jit(solution)/shard_map/all_to_all | solution.py:211
  206.9 3.2 %fusion.99 = f32[256,512]{1,0:T(8,128)} fusion(bf16[2048,512]{1,0:T(8,128)(2,1)} %param.33, bf16[256,2048]{1,0:T(8,128)(2,1)S(1)} %copy-done.3, f32[2048]{0:T(1024)S(1)} %copy-done.11, f32[256]{0:T(256)S(1)} %add_rsqrt_fusion), kind=kOutput, calls=%fused_computation.145 | convolution fusion | flops 538968064 | bytes 3679232 | tf_op jit(solution)/shard_map/dot_general | solution.py:179
  210.1 42.6 %all-to-all-done.3 = bf16[16,48,2048]{2,1,0:T(8,128)(2,1)} async-done(((bf16[16,48,2048]{2,1,0:T(8,128)(2,1)}), bf16[16,48,2048]{2,1,0:T(8,128)(2,1)}, u32[]{:S(2)}, u32[]{:S(2)}) %all-to-all-start.3) | async-done | bytes 3145760 | tf_op jit(solution)/shard_map/all_to_all | solution.py:211
  252.7 7.6 %gather_fusion.1 = bf16[512,2048]{1,0:T(8,128)(2,1)} fusion(bf16[768,2048]{1,0:T(8,128)(2,1)} %bitcast.22, s32[1024]{0:T(1024)S(1)} %pad_clamp_fusion), kind=kCustom, calls=%fused_computation.1 | custom fusion | bytes 4196352 | tf_op jit(solution)/shard_map/gather | solution.py:212
  260.2 5.4 %reshape.495 = f32[256,2,2048]{2,1,0:T(2,128)} reshape(bf16[512,2048]{1,0:T(8,128)(2,1)} %gather_fusion.1) | data formatting | bytes 6291456 | tf_op jit(solution)/shard_map/convert_element_type | solution.py:212
  265.7 10.1 %multiply_reduce_fusion = f32[256,2048]{1,0:T(8,128)} fusion(f32[256,2,2048]{2,1,0:T(2,128)} %reshape.495, f32[256,2]{1,0:T(8,128)S(1)} %copy.60), kind=kLoop, calls=%fused_computation.57 | loop fusion | flops 1572864 | bytes 6293504 | tf_op jit(solution)/shard_map/reduce_sum | solution.py:214
  275.8 4.8 %fusion.53 = bf16[256,2048]{1,0:T(8,128)(2,1)} fusion(bf16[2048,512]{1,0:T(8,128)(2,1)S(1)} %copy-done, f32[256,2048]{1,0:T(8,128)} %multiply_reduce_fusion, bf16[256,2048]{1,0:T(8,128)(2,1)S(1)} %copy-done.3, bf16[2048,512]{1,0:T(8,128)(2,1)} %param.34, f32[256,512]{1,0:T(8,128)} %fusion.99, f32[2048]{0:T(1024)S(1)} %copy-done.11, f32[256]{0:T(256)S(1)} %add_rsqrt_fusion), kind=kOutput, calls=%fused_computation.65 | convolution fusion | flops 1078722560 | bytes 8922112 | tf_op jit(solution)/shard_map/dot_general | solution.py:182
  (188 shorter events, 35.2 us)
Async XLA Ops:
  6.5 269.3 %copy-start = (bf16[2048,512]{1,0:T(8,128)(2,1)S(1)}, bf16[2048,512]{1,0:T(8,128)(2,1)}, u32[]{:S(2)}) copy-start(bf16[2048,512]{1,0:T(8,128)(2,1)} %param.35) | copy-start | bytes 6291460
  6.5 2.9 copy-start.9
  6.5 6.2 %copy-start.5 = (bf16[4096,64]{0,1:T(8,128)(2,1)S(1)}, bf16[4096,64]{0,1:T(8,128)(2,1)}, u32[]{:S(2)}) copy-start(bf16[4096,64]{0,1:T(8,128)(2,1)} %param.20) | copy-start | bytes 1572868
  6.5 6.2 %copy-start.6 = (bf16[4096,64]{0,1:T(8,128)(2,1)S(1)}, bf16[4096,64]{0,1:T(8,128)(2,1)}, u32[]{:S(2)}) copy-start(bf16[4096,64]{0,1:T(8,128)(2,1)} %param.21) | copy-start | bytes 1572868
  6.5 124.2 %all-gather.3.cloned.1.call-start = ((), (), s32[]{:S(2)}) async-start(), calls=%async_computation.4 | async-start | bytes 4456448 | tf_op jit(solution)/shard_map/all_gather | solution.py:145
  7.3 178.2 %all-gather.5.cloned.1.call-start = ((), (), s32[]{:S(2)}) async-start(), calls=%async_computation.5 | async-start | bytes 13369344 | tf_op jit(solution)/shard_map/all_gather | solution.py:61
  9.4 12.7 %copy-start.12 = (s32[256,2]{0,1:T(2,128)S(1)}, s32[256,2]{0,1:T(2,128)}, u32[]{:S(2)}) copy-start(s32[256,2]{0,1:T(2,128)} %param.28) | copy-start | bytes 6148
  14.4 18.1 %all-to-all-start = ((f32[16,65,64]{1,2,0:T(8,128)}), f32[16,65,64]{1,2,0:T(8,128)}, u32[]{:S(2)}, u32[]{:S(2)}) async-start(f32[16,65,64]{1,2,0:T(8,128)} %broadcast_in_dim.39), calls=%async_computation | async-start | bytes 1048576 | tf_op jit(solution)/shard_map/all_to_all | solution.py:15
  22.5 2.3 copy-start.7
  22.5 3.4 %copy-start.8 = (bf16[4096,64]{0,1:T(8,128)(2,1)S(1)}, bf16[4096,64]{0,1:T(8,128)(2,1)}, u32[]{:S(2)}) copy-start(bf16[4096,64]{0,1:T(8,128)(2,1)} %param.19) | copy-start | bytes 1572868
  28.5 10.4 %copy-start.10 = (s32[16,5]{0,1:T(8,128)}, s32[16,5]{0,1:T(8,128)S(1)}, u32[]{:S(2)}) copy-start(s32[16,5]{0,1:T(8,128)S(1)} %reduce-window.27) | copy-start | bytes 964
  95.4 0.7 copy-start.14
  95.6 1.0 copy-start.4
  96.6 12.1 %slice-start = ((s32[16,5]{0,1:T(8,128)}), s32[16,4]{0,1:T(4,128)S(1)}, s32[]{:S(2)}) async-start(s32[16,5]{0,1:T(8,128)} %copy-done.10), calls=%async_computation.6 | async-start | bytes 4096 | tf_op jit(solution)/shard_map/slice.5
  97.9 32.8 %all-to-all-start.1 = ((bf16[16,256,64]{1,2,0:T(8,128)(2,1)}), bf16[16,256,64]{1,2,0:T(8,128)(2,1)S(1)}, u32[]{:S(2)}, u32[]{:S(2)}) async-start(bf16[16,256,64]{1,2,0:T(8,128)(2,1)} %bitcast.155), calls=%async_computation.1 | async-start | bytes 1048576 | tf_op jit(solution)/shard_map/all_to_all | solution.py:169
  130.7 5.0 %copy-start.11 = (f32[2048]{0:T(1024)S(1)}, f32[2048]{0:T(1024)}, u32[]{:S(2)}) copy-start(f32[2048]{0:T(1024)} %param.27) | copy-start | bytes 24580
  134.8 1.0 copy-start.2
  185.5 6.4 %copy-start.1 = (bf16[16,48,2048]{2,1,0:T(8,128)(2,1)S(1)}, bf16[16,48,2048]{2,1,0:T(8,128)(2,1)}, u32[]{:S(2)}) copy-start(bf16[16,48,2048]{2,1,0:T(8,128)(2,1)} %all_to_all.34) | copy-start | bytes 9437188
  185.5 7.7 %copy-start.15 = (bf16[6144,1024]{0,1:T(8,128)(2,1)S(1)}, bf16[6144,1024]{0,1:T(8,128)(2,1)}, u32[]{:S(2)}) copy-start(bf16[6144,1024]{0,1:T(8,128)(2,1)} %all-gather.5.cloned.1.call-done) | copy-start | bytes 37748740
  201.9 4.8 %copy-start.13 = (f32[256,2]{0,1:T(2,128)S(1)}, f32[256,2]{0,1:T(2,128)}, u32[]{:S(2)}) copy-start(f32[256,2]{0,1:T(2,128)} %param.29) | copy-start | bytes 6148
  201.9 5.0 %copy-start.3 = (bf16[256,2048]{1,0:T(8,128)(2,1)S(1)}, bf16[256,2048]{1,0:T(8,128)(2,1)}, u32[]{:S(2)}) copy-start(bf16[256,2048]{1,0:T(8,128)(2,1)} %copy-done.2) | copy-start | bytes 3145732
  201.9 50.8 %all-to-all-start.3 = ((bf16[16,48,2048]{2,1,0:T(8,128)(2,1)}), bf16[16,48,2048]{2,1,0:T(8,128)(2,1)}, u32[]{:S(2)}, u32[]{:S(2)}) async-start(bf16[16,48,2048]{2,1,0:T(8,128)(2,1)} %bitcast.197), calls=%async_computation.3 | async-start | bytes 6291456 | tf_op jit(solution)/shard_map/all_to_all | solution.py:211
Sparse Core Ops, SparseCore 0:
  9.1 53.0 all-gather.2
  64.0 85.5 all-gather.4
where the time goes:
time: 290 us; the launch traced here: 287 us
  waiting for transfers between devices  62.7 us (22%)
  matrix products  57.1 us (20%)
  local copies, waits for them, and re-layouts  51.3 us (18%)
  blocking collectives  42.9 us (15%)
  other arithmetic  24.2 us (8%)
  starting transfers between devices  23.1 us (8%)
  between operations  15.1 us (5%)
  loops' own time  11 us (4%)
    all_to_all x1, blocking collectives, on_device(): lax.all_to_all(outgoing, 'sp', split_axis=0, concat_axis=0, tiled=True)  42.9 us
    all_to_all x1, waiting for transfers between devices, on_device(): lax.all_to_all(processed, 'sp', split_axis=0, concat_axis=0, tiled=True)  42.6 us
    all_to_all x1, waiting for transfers between devices, on_device(): lax.all_to_all(ret_rows, 'tp', split_axis=0, concat_axis=1, tiled=True)  15.4 us
    dot_general x8, matrix products, advance(): jnp.einsum('svc,csj->vsj', decay_weighted, block_values, preferred_elemen...  11.7 us
    another operation x1, loops' own time, block_pass(): lax.scan(advance, state, (query_blocks, key_blocks, value_blocks, decay_b...  11 us
    all_to_all x1, starting transfers between devices, on_device(): lax.all_to_all(ret_rows, 'tp', split_axis=0, concat_axis=1, tiled=True)  10.5 us
    reduce_sum x1, other arithmetic, on_device(): jnp.sum(decay_weighted.reshape(token_count, chosen_count, model_width), a...  10.1 us
    slice x16, local copies, waits for them, and re-layouts, advance(): carry = carry * jnp.exp(running[:, -1])[:, None, None] + state_update  9.42 us
  transfers between devices with their start and end apart: 5, of which 3 were waited for; matrix products, arithmetic and copies ran while one was open for 30% of the time, Pallas kernels for 0%

commit v1 on v0

v1 whole, which is shorter than its diff:
```python
import functools

import jax
import jax.numpy as jnp
from jax import lax
from jax.experimental import pallas as pl
from jax.experimental.pallas import tpu as pltpu
from jax.sharding import PartitionSpec as P

HEAD = 64
SPAN = 512
EPS = 1e-05
SCALE = HEAD ** (-0.5)
CHUNKS = 2

f32 = jnp.float32
bf16 = jnp.bfloat16


def split3(x):
    hi = x.astype(bf16)
    rest = x - hi.astype(f32)
    mid = rest.astype(bf16)
    return hi, mid, (rest - mid.astype(f32)).astype(bf16)


def dot(a, b, dims):
    return lax.dot_general(a, b, (dims, ((), ())), preferred_element_type=f32)


def running_sum(x):
    lane = lax.broadcasted_iota(jnp.int32, x.shape, 1)
    shift = 1
    while shift < x.shape[1]:
        x = x + jnp.where(lane >= shift, pltpu.roll(x, shift, 1), 0.0)
        shift *= 2
    return x


def state_kernel(decay_ref, k_ref, v_ref, packed_ref, prefix_ref, run_ref):
    count = decay_ref.shape[1] // SPAN
    run = running_sum(
        jnp.concatenate(
            [decay_ref[:, b * SPAN : (b + 1) * SPAN] for b in range(count)], axis=0
        )
    )
    run_ref[...] = run
    ends = run[:, SPAN - 1 :]
    weight = jnp.exp(ends - run) * SCALE
    state = jnp.zeros((HEAD, HEAD), f32)
    total = jnp.zeros((1, 1), f32)
    for b in range(count):
        prefix_ref[b] = state
        cols = slice(b * SPAN, (b + 1) * SPAN)
        scaled = k_ref[:, cols].astype(f32) * weight[b : b + 1]
        vals = v_ref[:, cols]
        update = sum(dot(vals, part, ((1,), (1,))) for part in split3(scaled))
        state = state * jnp.exp(ends[b : b + 1]) + update
        total = total + ends[b : b + 1]
    half = HEAD // 2
    packed_ref[0:half, :] = jnp.concatenate([state[:half], state[half:]], axis=1)
    packed_ref[half:, :] = jnp.broadcast_to(jnp.exp(total), (8, 2 * HEAD))


def inner_kernel(run_ref, q_ref, k_ref, v_ref, out_ref):
    count = run_ref.shape[0]
    run = run_ref[...]
    run_cols = run.T
    part = SPAN // 2
    for b in range(count):
        base = b * SPAN
        keys = k_ref[:, base : base + SPAN].T
        for j in range(2):
            depth = (j + 1) * part
            scores = dot(
                keys[:depth],
                q_ref[:, base + j * part : base + depth],
                ((1,), (0,)),
            )
            spread = (
                run[b : b + 1, j * part : depth] - run_cols[:depth, b : b + 1]
            )
            earlier = lax.broadcasted_iota(jnp.int32, (depth, part), 0)
            later = lax.broadcasted_iota(jnp.int32, (depth, part), 1) + j * part
            damping = jnp.exp(jnp.where(earlier <= later, spread, -jnp.inf))
            weighted = (scores * SCALE * damping).astype(bf16)
            out_ref[:, base + j * part : base + depth] = dot(
                v_ref[:, base : base + depth], weighted, ((1,), (0,))
            )


def finish_kernel(
    place_ref, all_ref, prefix_ref, run_ref, inner_ref, q_ref, g_ref, gain_ref, out_ref
):
    place = place_ref[0]
    half = HEAD // 2
    packed = jnp.zeros((half, 2 * HEAD), f32)
    for i in range(all_ref.shape[0]):
        joined = packed * all_ref[i, half : half + 1, :] + all_ref[i, :half, :]
        packed = jnp.where(i < place, joined, packed)
    incoming = jnp.concatenate([packed[:, :HEAD], packed[:, HEAD:]], axis=0)
    run = run_ref[...]
    grow = jnp.exp(run)
    ends = run[:, SPAN - 1 :]
    row = lax.broadcasted_iota(jnp.int32, (HEAD, HEAD), 0)
    col = lax.broadcasted_iota(jnp.int32, (HEAD, HEAD), 1)
    gain = jnp.sum(
        jnp.where(row == col, jnp.broadcast_to(gain_ref[...], (HEAD, HEAD)), 0.0),
        axis=1,
        keepdims=True,
    )
    base = jnp.zeros((1, 1), f32)
    part = out_ref.shape[2]
    for b in range(run.shape[0]):
        cols = slice(b * SPAN, (b + 1) * SPAN)
        entering = prefix_ref[b] + jnp.exp(base) * incoming
        queries = q_ref[:, cols]
        carried = sum(dot(piece, queries, ((1,), (0,))) for piece in split3(entering))
        retained = inner_ref[:, cols] + carried * grow[b : b + 1]
        centered = retained - jnp.mean(retained, axis=0, keepdims=True)
        spread = jnp.mean(centered * centered, axis=0, keepdims=True)
        gate = g_ref[:, cols].astype(f32)
        rows = (
            centered * lax.rsqrt(spread + EPS) * gain * (gate * jax.nn.sigmoid(gate))
        ).astype(bf16)
        for i in range(SPAN // part):
            out_ref[b * (SPAN // part) + i] = rows[:, i * part : (i + 1) * part]
        base = base + ends[b : b + 1]


def mix_kernel(x_ref, w_ref, res_ref, gain_ref, slot_ref, hidden_ref, normed_ref, *outs):
    tokens, width = res_ref.shape
    cut = 2 * w_ref.shape[2]
    x = x_ref[...].T
    squares = jnp.zeros((tokens, 1), f32)
    for p in range(width // cut):
        cols = slice(p * cut, (p + 1) * cut)
        weight = jnp.concatenate([w_ref[2 * p], w_ref[2 * p + 1]], axis=1)
        mixed = dot(x, weight, ((1,), (0,)))
        hidden = (res_ref[:, cols].astype(f32) + mixed).astype(bf16)
        hidden_ref[:, cols] = hidden
        wide = hidden.astype(f32)
        squares = squares + jnp.sum(wide * wide, axis=1, keepdims=True)
    scale = lax.rsqrt(squares * (1.0 / width) + EPS)
    picks = []
    for c, out_ref in enumerate(outs):
        rows = out_ref.shape[0]
        index = lax.broadcasted_iota(jnp.int32, (rows, tokens), 0) + c * rows
        hit = (index == slot_ref[0:1, :]) | (index == slot_ref[1:2, :])
        picks.append(jnp.where(hit, 1.0, 0.0).astype(bf16))
    for p in range(width // cut):
        cols = slice(p * cut, (p + 1) * cut)
        normed = (
            hidden_ref[:, cols].astype(f32) * scale * gain_ref[:, cols]
        ).astype(bf16)
        normed_ref[:, cols] = normed
        for pick, out_ref in zip(picks, outs):
            out_ref[:, cols] = dot(pick, normed, ((1,), (0,))).astype(bf16)


def call(kernel, outs, args, flops, name, smem=()):
    def full(place):
        return pl.BlockSpec(memory_space=pltpu.SMEM if place in smem else pltpu.VMEM)

    moved = sum(a.size * a.dtype.itemsize for a in (*args, *outs))
    return pl.pallas_call(
        kernel,
        out_shape=outs,
        in_specs=[full(k) for k in range(len(args))],
        out_specs=[pl.BlockSpec(memory_space=pltpu.VMEM) for _ in outs],
        cost_estimate=pl.CostEstimate(flops=flops, bytes_accessed=moved, transcendentals=0),
        compiler_params=pltpu.CompilerParams(vmem_limit_bytes=48 * 1024 * 1024),
        name=name,
    )(*args)


def on_device(
    query_rows,
    key_rows,
    value_rows,
    gate_rows,
    log_decay,
    residual,
    head_gain,
    out_weight,
    norm_gain,
    expert_ids,
    route_weights,
    expert_gate,
    expert_up,
    expert_down,
    shared_gate,
    shared_up,
    shared_down,
):
    shape = jax.ShapeDtypeStruct
    seq_rows, local_width = query_rows.shape
    tokens, width = residual.shape
    experts = lax.axis_size("sp")
    columns = lax.axis_size("tp")
    blocks = seq_rows // SPAN
    out_full = lax.all_gather(out_weight, "tp", axis=0, tiled=False)
    gate_full = lax.all_gather(expert_gate.T, "tp", axis=0, tiled=True)
    up_full = lax.all_gather(expert_up.T, "tp", axis=0, tiled=True)
    down_full = lax.all_gather(expert_down.T, "tp", axis=0, tiled=True)

    queries, keys, values, gates = (a.T for a in (query_rows, key_rows, value_rows, gate_rows))
    packed, prefix, run = call(
        state_kernel,
        [
            shape((HEAD // 2 + 8, 2 * HEAD), f32),
            shape((blocks, HEAD, HEAD), f32),
            shape((blocks, SPAN), f32),
        ],
        [log_decay, keys, values],
        6 * seq_rows * HEAD * HEAD,
        "states",
    )
    everyone = lax.all_to_all(
        jnp.broadcast_to(packed[None], (experts, *packed.shape)), "sp", 0, 0, tiled=True
    )
    (inner,) = call(
        inner_kernel,
        [shape((HEAD, seq_rows), f32)],
        [run, queries, keys, values],
        4 * seq_rows * HEAD * SPAN,
        "inner",
    )
    place = lax.axis_index("sp").astype(jnp.int32).reshape(1)
    (ret_rows,) = call(
        finish_kernel,
        [shape((columns, HEAD, seq_rows // columns), bf16)],
        [place, everyone, prefix, run, inner, queries, gates, head_gain.reshape(1, -1)],
        6 * seq_rows * HEAD * HEAD,
        "finish",
        smem=(0,),
    )
    token_rows = lax.all_to_all(ret_rows, "tp", 0, 0, tiled=True)

    capacity = 3 * tokens * 2 // (2 * experts)
    share = capacity // CHUNKS
    ids = expert_ids.T
    each = jnp.arange(experts, dtype=jnp.int32)[:, None]
    named = [each == ids[j : j + 1] for j in range(2)]
    member = (named[0] | named[1]).astype(bf16)
    before = jnp.triu(jnp.ones((tokens, tokens), bf16), 1)
    position = jnp.dot(member, before, preferred_element_type=f32).astype(jnp.int32)
    spot = (position // share) * (experts * share) + each * share + position % share
    slots = jnp.stack([jnp.sum(jnp.where(n, spot, 0), axis=0) for n in named])

    rows = experts * share
    hidden, normed, *outgoing = call(
        mix_kernel,
        [shape((tokens, width), bf16)] * 2 + [shape((rows, width), bf16)] * CHUNKS,
        [
            token_rows.reshape(columns * HEAD, tokens),
            out_full,
            residual,
            norm_gain.reshape(1, -1),
            slots,
        ],
        2 * tokens * width * (columns * HEAD + rows * CHUNKS),
        "mix",
    )
    routing = route_weights.T
    routed = None
    for c in range(CHUNKS):
        arrived = lax.all_to_all(
            outgoing[c].reshape(experts, share, width), "sp", 0, 0, tiled=True
        ).reshape(rows, width)
        middle = (
            jax.nn.silu(dot(arrived, gate_full, ((1,), (1,))))
            * dot(arrived, up_full, ((1,), (1,)))
        ).astype(bf16)
        outcome = dot(middle, down_full, ((1,), (0,))).astype(bf16)
        returned = lax.all_to_all(
            outcome.reshape(experts, share, width), "sp", 0, 0, tiled=True
        ).reshape(rows, width)
        index = jnp.arange(rows, dtype=jnp.int32)[:, None] + c * rows
        spread = sum(
            jnp.where(index == slots[j : j + 1], routing[j : j + 1], 0.0) for j in range(2)
        )
        high = spread.astype(bf16)
        low = (spread - high.astype(f32)).astype(bf16)
        for piece in (high, low):
            term = dot(piece, returned, ((0,), (0,)))
            routed = term if routed is None else routed + term
    shared_mid = (
        jax.nn.silu(dot(normed, shared_gate, ((1,), (0,))))
        * dot(normed, shared_up, ((1,), (0,)))
    ).astype(bf16)
    shared_out = dot(shared_mid, shared_down, ((1,), (1,)))
    return (hidden.astype(f32) + routed + shared_out).astype(bf16)


def solution(mesh):
    placed = (
        P("sp", "tp"),
        P("sp", "tp"),
        P("sp", "tp"),
        P("sp", "tp"),
        P("tp", "sp"),
        P(("sp", "tp"), None),
        P("tp"),
        P(None, "tp"),
        P(),
        P(("sp", "tp"), None),
        P(("sp", "tp"), None),
        P(None, ("sp", "tp")),
        P(None, ("sp", "tp")),
        P(None, ("sp", "tp")),
        P(),
        P(),
        P(),
    )
    return jax.shard_map(
        on_device, mesh=mesh, in_specs=placed, out_specs=P(("sp", "tp"), None), check_vma=False
    )
```

time: 290 us -> 278 us (0.959)
  waiting for transfers between devices: 62.7 us -> 124 us
  local copies, waits for them, and re-layouts: 51.3 us -> 14.4 us
  other arithmetic: 24.2 us -> 0.02 us
  blocking collectives: 42.9 us -> 27.7 us
  Pallas kernels: 0 us -> 11.4 us
  loops' own time: 11 us -> 0 us
  starting transfers between devices: 23.1 us -> 34 us
  matrix products: 57.1 us -> 50.3 us
    all_gather x2 -> x4, waiting for transfers between devices: 0.01 us -> 80.2 us  [the longest x1 42 us: on_device(): up_full = lax.all_gather(expert_up.T, 'tp', axis=0, tiled=True)]
    all_to_all x3 -> x5, waiting for transfers between devices: 62 us -> 41 us  [the longest x2 22.1 us: on_device(): lax.all_to_all(outcome.reshape(experts, share, width), 'sp', 0, 0, tiled=...]
    all_to_all x1, blocking collectives: 42.9 us -> 27.7 us  [on_device(): lax.all_to_all(outgoing[c].reshape(experts, share, width), 'sp', 0, 0, ti...]
    slice x34 -> x2, local copies, waits for them, and re-layouts: 14.7 us -> 0.01 us  [the longest x1 0.01 us: on_device(): named = [each == ids[j:j + 1] for j in range(2)]]
    gather x2 -> x0, local copies, waits for them, and re-layouts: 11.9 us -> none  [the longest x1 7.56 us: on_device(): returned.reshape(specialist_networks * capacity, model_width)[slot]]
    pallas_call x0 -> x4, Pallas kernels: none -> 11.4 us  [call(): pl.pallas_call(kernel, out_shape=outs, in_specs=[full(k) for k in range(l...]
    another operation x1 -> x0, loops' own time: 11 us -> none  [block_pass(): lax.scan(advance, state, (query_blocks, key_blocks, value_blocks, decay_b...]
    all_to_all x3 -> x5, starting transfers between devices: 23 us -> 33.9 us  [the longest x2 11.3 us: on_device(): lax.all_to_all(outcome.reshape(experts, share, width), 'sp', 0, 0, tiled=...]
  transfers between devices with their start and end apart: 5 -> 9, of which waited for: 3 -> 7; matrix products, arithmetic and copies ran while one was open for 30% -> 14% of each run, Pallas kernels for 0% -> 4%
where the time goes in v1:
time: 278 us; the launch traced here: 275 us
  waiting for transfers between devices  124 us (45%)
  matrix products  50.3 us (18%)
  starting transfers between devices  34 us (12%)
  blocking collectives  27.7 us (10%)
  local copies, waits for them, and re-layouts  14.4 us (5%)
  between operations  13.3 us (5%)
  Pallas kernels  11.4 us (4%)
    dot_general x10, matrix products, dot(): return lax.dot_general(a, b, (dims, ((), ())), preferred_element_type=f32)  50.1 us
    all_gather x1, waiting for transfers between devices, on_device(): up_full = lax.all_gather(expert_up.T, 'tp', axis=0, tiled=True)  42 us
    all_gather x1, waiting for transfers between devices, on_device(): down_full = lax.all_gather(expert_down.T, 'tp', axis=0, tiled=True)  36.8 us
    all_to_all x1, blocking collectives, on_device(): lax.all_to_all(outgoing[c].reshape(experts, share, width), 'sp', 0, 0, ti...  27.7 us
    all_to_all x2, waiting for transfers between devices, on_device(): lax.all_to_all(outcome.reshape(experts, share, width), 'sp', 0, 0, tiled=...  22.1 us
    all_to_all x1, waiting for transfers between devices, on_device(): token_rows = lax.all_to_all(ret_rows, 'tp', 0, 0, tiled=True)  16.9 us
    unnamed x40, local copies, waits for them, and re-layouts  13.6 us
    pallas_call x4, Pallas kernels, call(): pl.pallas_call(kernel, out_shape=outs, in_specs=[full(k) for k in range(l...  11.4 us
  transfers between devices with their start and end apart: 9, of which 7 were waited for; matrix products, arithmetic and copies ran while one was open for 14% of the time, Pallas kernels for 4%

profile of v1, /device:TPU:1, one launch (start us, length us, event | category | flops | bytes accessed | tf_op | source)
XLA Modules:
  0.0 275.0 jit_solution(7185443419019296569)
XLA Ops:
  6.5 0.7 all-gather.12.cloned.1.call-update
  7.3 0.0 all-gather.6.cloned.1.call-start
  7.3 0.7 all-gather.6.cloned.1.call-update
  8.1 0.7 all-gather.10.cloned.1.call-update
  8.8 0.5 all-gather.8.cloned.1.call-update
  9.3 1.0 copy-done.1
  10.4 1.0 copy-done.3
  11.4 0.7 copy-done.13
  12.1 1.2 states.1
  13.4 0.7 copy-done.11
  14.1 0.7 broadcast_in_dim.49
  14.8 7.7 %all-to-all-start = ((f32[16,40,128]{2,1,0:T(8,128)}), f32[16,40,128]{2,1,0:T(8,128)S(1)}, u32[]{:S(2)}, u32[]{:S(2)}) async-start(f32[16,40,128]{2,1,0:T(8,128)} %broadcast_in_dim.49), calls=%async_computation | async-start | bytes 655360 | tf_op jit(solution)/shard_map/all_to_all | solution.py:219
  22.5 1.0 copy-done.2
  23.6 1.1 copy-done.4
  24.7 1.0 copy-done.5
  25.7 3.2 %inner.1.inner_ref = f32[64,4096]{1,0:T(8,128)S(1)} custom-call(f32[8,512]{1,0:T(8,128)S(1)} %get-tuple-element.14.run_ref, bf16[64,4096]{1,0:T(8,128)(2,1)S(1)} %bitcast.51, bf16[64,4096]{1,0:T(8,128)(2,1)S(1)} %bitcast.48, bf16[64,4096]{1,0:T(8,128)(2,1)S(1)} %bitcast.50), custom_call_target="tpu_custom_call" | custom-call | flops 536870912 | bytes 2637824 | tf_op jit(solution)/shard_map/inner/pallas_call | solution.py:166
  29.0 2.1 all-to-all-done.all_ref
  31.1 1.1 copy-done.6
  32.1 1.0 copy-done.10
  33.2 0.9 copy-done.12
  34.1 1.0 finish.1
  35.1 0.8 copy-done.7
  35.9 10.3 %all-to-all-start.1 = ((bf16[16,64,256]{2,1,0:T(8,128)(2,1)}), bf16[16,64,256]{2,1,0:T(8,128)(2,1)S(1)}, u32[]{:S(2)}, u32[]{:S(2)}) async-start(bf16[16,64,256]{2,1,0:T(8,128)(2,1)} %copy-done.7), calls=%async_computation.1 | async-start | bytes 1048576 | tf_op jit(solution)/shard_map/all_to_all | solution.py:238
  46.2 0.2 select_reduce_fusion.1
  46.4 16.9 %all-to-all-done.1 = bf16[16,64,256]{2,1,0:T(8,128)(2,1)S(1)} async-done(((bf16[16,64,256]{2,1,0:T(8,128)(2,1)}), bf16[16,64,256]{2,1,0:T(8,128)(2,1)S(1)}, u32[]{:S(2)}, u32[]{:S(2)}) %all-to-all-start.1) | async-done | bytes 524320 | tf_op jit(solution)/shard_map/all_to_all | solution.py:238
  63.3 0.8 copy-done.8
  64.1 1.0 copy-done.9
  65.1 1.2 copy-done.15
  66.3 5.9 %mix.1 = (bf16[256,2048]{1,0:T(8,128)(2,1)S(1)}, bf16[256,2048]{1,0:T(8,128)(2,1)S(1)}, bf16[384,2048]{1,0:T(8,128)(2,1)S(1)}, bf16[384,2048]{1,0:T(8,128)(2,1)}) custom-call(bf16[1024,256]{1,0:T(8,128)(2,1)S(1)} %bitcast.54, bf16[16,1024,128]{2,1,0:T(8,128)(2,1)} %bitcast.80, bf16[256,2048]{1,0:T(8,128)(2,1)S(1)} %copy-done.15, f32[1,2048]{1,0:T(1,128)S(1)} %bitcast.57, ...), custom_call_target="tpu_custom_call" | custom-call | flops 1879048192 | bytes 11020288 | tf_op jit(solution)/shard_map/mix/pallas_call | solution.py:166
  72.3 27.7 %all_to_all.30 = bf16[16,24,2048]{2,1,0:T(8,128)(2,1)} all-to-all(bf16[16,24,2048]{2,1,0:T(8,128)(2,1)S(1)} %bitcast.53), channel_id=1, replica_groups=mesh['sp'=16,'tp'=16] {'sp'}, dimensions={0} | all-to-all | bytes 3145728 | tf_op jit(solution)/shard_map/all_to_all | solution.py:268
  100.0 4.6 %all-to-all-start.4 = ((bf16[16,24,2048]{2,1,0:T(8,128)(2,1)}), bf16[16,24,2048]{2,1,0:T(8,128)(2,1)}, u32[]{:S(2)}, u32[]{:S(2)}) async-start(bf16[16,24,2048]{2,1,0:T(8,128)(2,1)} %bitcast.58), calls=%async_computation.4 | async-start | bytes 3145728 | tf_op jit(solution)/shard_map/all_to_all | solution.py:268
  104.6 1.4 all-gather.6.cloned.1.call-done
  106.0 5.6 %fusion.54 = f32[384,1024]{1,0:T(8,128)} fusion(bf16[384,2048]{1,0:T(8,128)(2,1)} %bitcast.61, bf16[1024,2048]{1,0:T(8,128)(2,1)} %all-gather.6.cloned.1.call-done), kind=kOutput, calls=%fused_computation.72 | convolution fusion | flops 1610612736 | bytes 7340032 | tf_op jit(solution)/shard_map/dot_general | solution.py:28
  111.7 36.8 %all-gather.10.cloned.1.call-done = bf16[1024,2048]{1,0:T(8,128)(2,1)} async-done(((bf16[64,2048]{1,0:T(8,128)(2,1)}), bf16[1024,2048]{1,0:T(8,128)(2,1)}) %all-gather.10.cloned.1.call-update) | async-done | bytes 4194320 | tf_op jit(solution)/shard_map/all_gather | solution.py:205
  148.5 42.0 %all-gather.8.cloned.1.call-done = bf16[1024,2048]{1,0:T(8,128)(2,1)} async-done(((bf16[64,2048]{1,0:T(8,128)(2,1)}), bf16[1024,2048]{1,0:T(8,128)(2,1)}) %all-gather.8.cloned.1.call-update) | async-done | bytes 4194320 | tf_op jit(solution)/shard_map/all_gather | solution.py:204
  190.5 9.1 %convolution_convert_fusion.1 = bf16[384,2048]{1,0:T(8,128)(2,1)} fusion(bf16[1024,2048]{1,0:T(8,128)(2,1)} %all-gather.10.cloned.1.call-done, f32[384,1024]{1,0:T(8,128)} %fusion.54, bf16[384,2048]{1,0:T(8,128)(2,1)} %bitcast.62, bf16[1024,2048]{1,0:T(8,128)(2,1)} %all-gather.8.cloned.1.call-done), kind=kOutput, calls=%fused_computation.1 | convolution fusion | flops 3224371200 | bytes 13107200 | tf_op jit(solution)/shard_map/dot_general | solution.py:28
  199.6 6.6 %all-to-all-start.3 = ((bf16[16,24,2048]{2,1,0:T(8,128)(2,1)}), bf16[16,24,2048]{2,1,0:T(8,128)(2,1)}, u32[]{:S(2)}, u32[]{:S(2)}) async-start(bf16[16,24,2048]{2,1,0:T(8,128)(2,1)} %bitcast.60), calls=%async_computation.3 | async-start | bytes 3145728 | tf_op jit(solution)/shard_map/all_to_all | solution.py:276
  206.2 5.7 %fusion.55 = f32[384,1024]{1,0:T(8,128)} fusion(bf16[384,2048]{1,0:T(8,128)(2,1)} %bitcast.25, bf16[1024,2048]{1,0:T(8,128)(2,1)} %all-gather.6.cloned.1.call-done), kind=kOutput, calls=%fused_computation.73 | convolution fusion | flops 1610612736 | bytes 7340032 | tf_op jit(solution)/shard_map/dot_general | solution.py:28
  211.8 9.1 %convolution_convert_fusion = bf16[384,2048]{1,0:T(8,128)(2,1)} fusion(bf16[1024,2048]{1,0:T(8,128)(2,1)} %all-gather.10.cloned.1.call-done, f32[384,1024]{1,0:T(8,128)} %fusion.55, bf16[384,2048]{1,0:T(8,128)(2,1)} %bitcast.25, bf16[1024,2048]{1,0:T(8,128)(2,1)} %all-gather.8.cloned.1.call-done), kind=kOutput, calls=%fused_computation | convolution fusion | flops 3224371200 | bytes 13107200 | tf_op jit(solution)/shard_map/dot_general | solution.py:28
  220.9 9.9 %all-to-all-done.3 = bf16[16,24,2048]{2,1,0:T(8,128)(2,1)} async-done(((bf16[16,24,2048]{2,1,0:T(8,128)(2,1)}), bf16[16,24,2048]{2,1,0:T(8,128)(2,1)}, u32[]{:S(2)}, u32[]{:S(2)}) %all-to-all-start.3) | async-done | bytes 1572896 | tf_op jit(solution)/shard_map/all_to_all | solution.py:276
  230.8 4.8 %all-to-all-start.5 = ((bf16[16,24,2048]{2,1,0:T(8,128)(2,1)}), bf16[16,24,2048]{2,1,0:T(8,128)(2,1)}, u32[]{:S(2)}, u32[]{:S(2)}) async-start(bf16[16,24,2048]{2,1,0:T(8,128)(2,1)} %bitcast.59), calls=%async_computation.5 | async-start | bytes 3145728 | tf_op jit(solution)/shard_map/all_to_all | solution.py:276
  235.6 3.4 %fusion.56 = f32[256,512]{1,0:T(8,128)} fusion(bf16[256,2048]{1,0:T(8,128)(2,1)} %copy-done.17, bf16[2048,512]{1,0:T(8,128)(2,1)} %param.31), kind=kOutput, calls=%fused_computation.74 | convolution fusion | flops 536870912 | bytes 3670016 | tf_op jit(solution)/shard_map/dot_general | solution.py:28
  239.0 2.2 fusion.24
  241.2 3.5 %convolution_add_fusion.3 = f32[256,2048]{1,0:T(8,128)} fusion(f32[256,2048]{1,0:T(8,128)S(1)} %fusion.24, bf16[384,2048]{1,0:T(8,128)(2,1)} %bitcast.23, f32[256]{0:T(256)S(1)} %bitcast.73, s32[256]{0:T(256)S(1)} %get-tuple-element.20, f32[256]{0:T(256)S(1)} %bitcast.69, s32[256]{0:T(256)S(1)} %get-tuple-element.19), kind=kOutput, calls=%fused_computation.6 | convolution fusion | flops 404062208 | bytes 5771264 | tf_op jit(solution)/shard_map/dot_general | solution.py:28
  244.7 12.2 %all-to-all-done.5 = bf16[16,24,2048]{2,1,0:T(8,128)(2,1)} async-done(((bf16[16,24,2048]{2,1,0:T(8,128)(2,1)}), bf16[16,24,2048]{2,1,0:T(8,128)(2,1)}, u32[]{:S(2)}, u32[]{:S(2)}) %all-to-all-start.5) | async-done | bytes 1572896 | tf_op jit(solution)/shard_map/all_to_all | solution.py:276
  256.9 2.9 %convolution_add_fusion.2 = f32[256,2048]{1,0:T(8,128)S(1)} fusion(f32[256,2048]{1,0:T(8,128)} %convolution_add_fusion.3, bf16[384,2048]{1,0:T(8,128)(2,1)} %bitcast.27, f32[256]{0:T(256)S(1)} %bitcast.74, s32[256]{0:T(256)S(1)} %get-tuple-element.20, f32[256]{0:T(256)S(1)} %bitcast.70, s32[256]{0:T(256)S(1)} %get-tuple-element.19, s32[384]{0:T(512)S(1)} %iota_add_fusion), kind=kOutput, calls=%fused_computation.5 | convolution fusion | flops 403767296 | bytes 5772800 | tf_op jit(solution)/shard_map/dot_general | solution.py:28
  259.8 3.6 %fusion = f32[256,2048]{1,0:T(8,128)} fusion(f32[256,2048]{1,0:T(8,128)S(1)} %convolution_add_fusion.2, bf16[384,2048]{1,0:T(8,128)(2,1)} %bitcast.27, bf16[256,2048]{1,0:T(8,128)(2,1)S(1)} %get-tuple-element.15, f32[256]{0:T(256)S(1)} %bitcast.75, s32[256]{0:T(256)S(1)} %get-tuple-element.20, f32[256]{0:T(256)S(1)} %bitcast.71, ...), kind=kOutput, calls=%fused_computation.4 | convolution fusion | flops 405110784 | bytes 6821376 | tf_op jit(solution)/shard_map/dot_general | solution.py:28
  263.4 5.0 %fusion.1 = bf16[256,2048]{1,0:T(8,128)(2,1)} fusion(f32[256,2048]{1,0:T(8,128)} %fusion, bf16[2048,512]{1,0:T(8,128)(2,1)S(1)} %copy-done, bf16[256,2048]{1,0:T(8,128)(2,1)} %copy-done.17, bf16[2048,512]{1,0:T(8,128)(2,1)} %param.32, f32[256,512]{1,0:T(8,128)} %fusion.56), kind=kOutput, calls=%fused_computation.7 | convolution fusion | flops 1075576832 | bytes 8912896 | tf_op jit(solution)/shard_map/dot_general | solution.py:28
  (36 shorter events, 0.2 us)
Async XLA Ops:
  6.5 256.9 %copy-start = (bf16[2048,512]{1,0:T(8,128)(2,1)S(1)}, bf16[2048,512]{1,0:T(8,128)(2,1)}, u32[]{:S(2)}) copy-start(bf16[2048,512]{1,0:T(8,128)(2,1)} %param.33) | copy-start | bytes 6291460
  6.5 57.5 %all-gather.12.cloned.1.call-start = ((), (), s32[]{:S(2)}) async-start(), calls=%async_computation.9 | async-start | bytes 4456448 | tf_op jit(solution)/shard_map/all_gather | solution.py:202
  7.3 98.8 %all-gather.6.cloned.1.call-start = ((), (), s32[]{:S(2)}) async-start(), calls=%async_computation.6 | async-start | bytes 4456448 | tf_op jit(solution)/shard_map/all_gather | solution.py:203
  8.0 140.5 %all-gather.10.cloned.1.call-start = ((), (), s32[]{:S(2)}) async-start(), calls=%async_computation.8 | async-start | bytes 4456448 | tf_op jit(solution)/shard_map/all_gather | solution.py:205
  8.7 181.7 %all-gather.8.cloned.1.call-start = ((), (), s32[]{:S(2)}) async-start(), calls=%async_computation.7 | async-start | bytes 4456448 | tf_op jit(solution)/shard_map/all_gather | solution.py:204
  9.3 1.0 copy-start.1
  10.4 1.0 copy-start.3
  11.4 0.7 copy-start.13
  13.4 0.7 copy-start.11
  14.8 16.2 %copy-start.14 = (f32[64]{0:T(128)S(1)}, f32[64]{0:T(128)}, u32[]{:S(2)}) copy-start(f32[64]{0:T(128)} %param.23) | copy-start | bytes 772
  14.8 16.2 %all-to-all-start = ((f32[16,40,128]{2,1,0:T(8,128)}), f32[16,40,128]{2,1,0:T(8,128)S(1)}, u32[]{:S(2)}, u32[]{:S(2)}) async-start(f32[16,40,128]{2,1,0:T(8,128)} %broadcast_in_dim.49), calls=%async_computation | async-start | bytes 655360 | tf_op jit(solution)/shard_map/all_to_all | solution.py:219
  22.5 1.0 copy-start.2
  23.6 1.1 copy-start.4
  24.7 1.0 copy-start.5
  31.1 1.1 copy-start.6
  32.1 1.0 copy-start.10
  33.1 0.9 copy-start.12
  34.1 12.1 %copy-start.18 = (s32[256,2]{0,1:T(2,128)S(1)}, s32[256,2]{0,1:T(2,128)}, u32[]{:S(2)}) copy-start(s32[256,2]{0,1:T(2,128)} %param.26) | copy-start | bytes 6148
  34.1 30.0 %copy-start.16 = (f32[2048]{0:T(1024)S(1)}, f32[2048]{0:T(1024)}, u32[]{:S(2)}) copy-start(f32[2048]{0:T(1024)} %param.25) | copy-start | bytes 24580
  35.1 0.8 copy-start.7
  35.9 27.4 %all-to-all-start.1 = ((bf16[16,64,256]{2,1,0:T(8,128)(2,1)}), bf16[16,64,256]{2,1,0:T(8,128)(2,1)S(1)}, u32[]{:S(2)}, u32[]{:S(2)}) async-start(bf16[16,64,256]{2,1,0:T(8,128)(2,1)} %copy-done.7), calls=%async_computation.1 | async-start | bytes 1048576 | tf_op jit(solution)/shard_map/all_to_all | solution.py:238
  63.3 0.8 copy-start.8
  64.1 1.0 copy-start.9
  65.1 1.2 copy-start.15
  72.3 27.7 %copy-start.17 = (bf16[256,2048]{1,0:T(8,128)(2,1)}, bf16[256,2048]{1,0:T(8,128)(2,1)S(1)}, u32[]{:S(2)}) copy-start(bf16[256,2048]{1,0:T(8,128)(2,1)S(1)} %get-tuple-element.18) | copy-start | bytes 3145732
  100.0 99.6 %all-to-all-start.4 = ((bf16[16,24,2048]{2,1,0:T(8,128)(2,1)}), bf16[16,24,2048]{2,1,0:T(8,128)(2,1)}, u32[]{:S(2)}, u32[]{:S(2)}) async-start(bf16[16,24,2048]{2,1,0:T(8,128)(2,1)} %bitcast.58), calls=%async_computation.4 | async-start | bytes 3145728 | tf_op jit(solution)/shard_map/all_to_all | solution.py:268
  199.6 31.2 %all-to-all-start.3 = ((bf16[16,24,2048]{2,1,0:T(8,128)(2,1)}), bf16[16,24,2048]{2,1,0:T(8,128)(2,1)}, u32[]{:S(2)}, u32[]{:S(2)}) async-start(bf16[16,24,2048]{2,1,0:T(8,128)(2,1)} %bitcast.60), calls=%async_computation.3 | async-start | bytes 3145728 | tf_op jit(solution)/shard_map/all_to_all | solution.py:276
  230.8 4.8 %copy-start.19 = (f32[256,2]{0,1:T(2,128)S(1)}, f32[256,2]{0,1:T(2,128)}, u32[]{:S(2)}) copy-start(f32[256,2]{0,1:T(2,128)} %param.27) | copy-start | bytes 6148
  230.8 26.1 %all-to-all-start.5 = ((bf16[16,24,2048]{2,1,0:T(8,128)(2,1)}), bf16[16,24,2048]{2,1,0:T(8,128)(2,1)}, u32[]{:S(2)}, u32[]{:S(2)}) async-start(bf16[16,24,2048]{2,1,0:T(8,128)(2,1)} %bitcast.59), calls=%async_computation.5 | async-start | bytes 3145728 | tf_op jit(solution)/shard_map/all_to_all | solution.py:276
Sparse Core Ops, SparseCore 0:
  9.2 53.2 all-gather.11
  64.3 41.6 all-gather.5
  107.8 40.5 all-gather.9
  150.1 40.2 all-gather.7
